TPU v7x, 32 devices: a whole 2x2x4 slice. The times are simulated.
32 devices in a mesh: tp: 8 (over z, y), dp: 4 (over x, core).
Axes of the slice: x: 2, y: 2, z: 4, core: 2. Of those that a mesh axis runs over, the one named last changes fastest.
Arguments:
- stream: bfloat16 [256, 2048], P('tp', 'dp'), may hold values from -12 to 12
- norm_gain: float32 [2, 2048], P(None, 'dp'), may hold values from 0.1 to 1.9
- w_input: bfloat16 [2, 2048, 2048], P(None, 'dp', 'tp'), may hold values from -0.125 to 0.125
- lam_re: float32 [2, 128, 64], P(None, 'tp'), may hold values from -1 to -0.05
- lam_im: float32 [2, 128, 64], P(None, 'tp'), may hold values from 0 to 6
- log_dt: float32 [2, 128], P(None, 'tp'), may hold values from -3 to 0
- b_re: float32 [2, 128, 64, 16], P(None, 'tp'), may hold values from -1 to 1
- b_im: float32 [2, 128, 64, 16], P(None, 'tp'), may hold values from -1 to 1
- readout_real: float32 [2, 128, 16, 64], P(None, 'tp'), may hold values from -0.5 to 0.5
- readout_imaginary: float32 [2, 128, 16, 64], P(None, 'tp'), may hold values from -0.5 to 0.5
- d_skip: float32 [2, 2048], P(None, 'tp'), may hold values from -4 to 4
- w_val: bfloat16 [2, 2048, 2048], P(None, 'tp', 'dp'), may hold values from -0.375 to 0.375
- w_gate: bfloat16 [2, 2048, 2048], P(None, 'tp', 'dp'), may hold values from -0.375 to 0.375
- state: float32 [2, 256, 128, 128], P(None, 'dp', 'tp'), may hold values from -6 to 6
Outputs:
- stream_out: bfloat16 [256, 2048], P('tp', 'dp')
- states_out: float32 [2, 256, 128, 128], P(None, 'dp', 'tp')
All inputs are finite; a program needn't handle non-finite values.
Results may differ from a plain program's by a relative error of at most 0.0064.
Values may be sent and summed in bfloat16 or wider, within the bound.
A program may use at most 64 MiB of HBM per device.

v0:
```python
import jax
import jax.numpy as jnp
from jax import lax
from jax.sharding import PartitionSpec as P

D = 2048
LAYERS = 2


eps = 1e-06


def advance(
    inputs, old_state, lam_re, lam_im, log_dt, b_re, b_im, readout_real, readout_imaginary, d_skip
):
    upper_bound = lax.Precision.HIGHEST
    count_rows, groups, doubled = old_state.shape
    half_state = doubled // 2
    chans = b_re.shape[-1]
    step_size = jnp.exp(log_dt)[:, None]
    decay = jnp.exp(lam_re * step_size)
    angle = lam_im * step_size
    keep_re = decay * jnp.cos(angle)
    keep_im = decay * jnp.sin(angle)
    denom = lam_re * lam_re + lam_im * lam_im
    ratio_re = ((keep_re - 1.0) * lam_re + keep_im * lam_im) / denom
    ratio_im = (keep_im * lam_re - (keep_re - 1.0) * lam_im) / denom
    drive_re = ratio_re[..., None] * b_re - ratio_im[..., None] * b_im
    drive_im = ratio_re[..., None] * b_im + ratio_im[..., None] * b_re
    grouped = inputs.reshape(count_rows, groups, chans)
    push_re = jnp.einsum("gpc,rgc->rgp", drive_re, grouped, precision=upper_bound)
    push_im = jnp.einsum("gpc,rgc->rgp", drive_im, grouped, precision=upper_bound)
    old_re = old_state[..., :half_state]
    old_im = old_state[..., half_state:]
    updated_real = keep_re * old_re - keep_im * old_im + push_re
    updated_imaginary = keep_re * old_im + keep_im * old_re + push_im
    readout_output = jnp.einsum(
        "aot,mat->mao", readout_real, updated_real, precision=upper_bound
    ) - jnp.einsum("aot,mat->mao", readout_imaginary, updated_imaginary, precision=upper_bound)
    pre_act = readout_output.reshape(count_rows, groups * chans) + d_skip * inputs
    return (pre_act, jnp.concatenate([updated_real, updated_imaginary], axis=-1))


def half_output(mixed_all, val_part, gate_part):
    return jnp.concatenate(
        [
            jnp.dot(mixed_all, val_part, preferred_element_type=jnp.float32),
            jnp.dot(mixed_all, gate_part, preferred_element_type=jnp.float32),
        ],
        axis=1,
    )


def per_device(
    stream,
    norm_gain,
    w_input,
    lam_re,
    lam_im,
    log_dt,
    b_re,
    b_im,
    readout_real,
    readout_imaginary,
    d_skip,
    w_val,
    w_gate,
    state,
):
    collected = []
    for layer_no in range(LAYERS):
        gathered = lax.all_gather(stream, "tp", axis=0, tiled=True)
        widened = gathered.astype(jnp.float32)
        normed = (widened * norm_gain[layer_no]).astype(jnp.bfloat16)
        square_part = jnp.sum(widened * widened, axis=1)
        weight_in = w_input[layer_no]
        partial_value = jnp.dot(normed, weight_in, preferred_element_type=jnp.float32)
        summed, square_total = (
            lax.psum_scatter(partial_value, "dp", scatter_dimension=0, tiled=True),
            lax.psum_scatter(square_part, "dp", scatter_dimension=0, tiled=True),
        )
        inputs = lax.rsqrt(square_total / D + eps)[:, None] * summed
        pre_act, new_state = advance(
            inputs,
            state[layer_no],
            lam_re[layer_no],
            lam_im[layer_no],
            log_dt[layer_no],
            b_re[layer_no],
            b_im[layer_no],
            readout_real[layer_no],
            readout_imaginary[layer_no],
            d_skip[layer_no],
        )
        mixed = jax.nn.gelu(pre_act).astype(jnp.bfloat16)
        mixed_all = lax.all_gather(mixed, "dp", axis=0, tiled=True)
        columns = w_val.shape[2]
        combined = lax.psum_scatter(
            half_output(mixed_all, w_val[layer_no], w_gate[layer_no]),
            "tp",
            scatter_dimension=0,
            tiled=True,
        )
        value = combined[:, :columns]
        gate = combined[:, columns:]
        stream = (stream.astype(jnp.float32) + value * jax.nn.sigmoid(gate)).astype(jnp.bfloat16)
        collected.append(new_state)
    return (stream, jnp.stack(collected))


def solution(mesh):
    return jax.shard_map(
        per_device,
        mesh=mesh,
        in_specs=(
            P("tp", "dp"),
            P(None, "dp"),
            P(None, "dp", "tp"),
            P(None, "tp", None),
            P(None, "tp", None),
            P(None, "tp"),
            P(None, "tp", None, None),
            P(None, "tp", None, None),
            P(None, "tp", None, None),
            P(None, "tp", None, None),
            P(None, "tp"),
            P(None, "tp", "dp"),
            P(None, "tp", "dp"),
            P(None, "dp", "tp", None),
        ),
        out_specs=(P("tp", "dp"), P(None, "dp", "tp", None)),
        check_vma=False,
    )
```

profile of v0, /device:TPU:14, one launch (start us, length us, event | category | flops | bytes accessed | tf_op | source)
XLA Modules:
  0.0 277.0 jit_solution(17151186009216203104)
XLA Ops:
  8.0 28.6 %all_gather.12 = bf16[256,512]{1,0:T(8,128)(2,1)S(1)} all-gather(bf16[32,512]{1,0:T(8,128)(2,1)} %param.14), channel_id=1, replica_groups=mesh['tp'=8,'dp'=4] {'tp'}, dimensions={0}, use_global_device_ids=true | all-gather | bytes 294912 | tf_op jit(solution)/shard_map/all_gather | solution.py:72
  36.6 1.9 fusion.10
  40.2 5.9 %all-reduce = f32[256]{0:T(256)S(1)} all-reduce(f32[256]{0:T(256)S(1)} %fusion.4), channel_id=2, replica_groups=mesh['tp'=8,'dp'=4] {'dp'}, use_global_device_ids=true, to_apply=%region_1.0.clone | all-reduce | flops 256 | bytes 2048
  48.5 12.8 %reduce-scatter.5.cloned.1.call-done = f32[64,256]{1,0:T(8,128)} async-done(((f32[256,256]{1,0:T(8,128)}), f32[64,256]{1,0:T(8,128)}) %reduce-scatter.5.cloned.1.call-update) | async-done | bytes 65552 | tf_op jit(solution)/shard_map/reduce_scatter | solution.py:79
  62.3 1.0 fusion.3
  63.4 1.0 fusion.2
  64.5 0.9 fusion.38
  65.4 0.9 convolution_subtract_fusion.1
  67.3 5.5 %all_gather.13 = bf16[256,256]{1,0:T(8,128)(2,1)S(1)} all-gather(bf16[64,256]{1,0:T(8,128)(2,1)S(1)} %fusion.63), channel_id=1, replica_groups=mesh['tp'=8,'dp'=4] {'dp'}, dimensions={0}, use_global_device_ids=true | all-gather | bytes 163840 | tf_op jit(solution)/shard_map/all_gather | solution.py:96
  73.3 1.1 pad_maximum_fusion
  74.5 65.0 %reduce-scatter.7.cloned.1.call-done = f32[32,1024]{1,0:T(8,128)} async-done(((f32[256,1024]{1,0:T(8,128)}), f32[32,1024]{1,0:T(8,128)}) %reduce-scatter.7.cloned.1.call-update) | async-done | bytes 131088 | tf_op jit(solution)/shard_map/reduce_scatter | solution.py:98
  140.4 26.5 %all_gather.14 = bf16[256,512]{1,0:T(8,128)(2,1)S(1)} all-gather(bf16[32,512]{1,0:T(8,128)(2,1)S(1)} %fusion.90), channel_id=1, replica_groups=mesh['tp'=8,'dp'=4] {'tp'}, dimensions={0}, use_global_device_ids=true | all-gather | bytes 294912 | tf_op jit(solution)/shard_map/all_gather | solution.py:72
  166.9 0.9 fusion.8
  168.0 5.8 %all-reduce.1 = f32[256]{0:T(256)S(1)} all-reduce(f32[256]{0:T(256)S(1)} %fusion.6), channel_id=5, replica_groups=mesh['tp'=8,'dp'=4] {'dp'}, use_global_device_ids=true, to_apply=%region_5.0.clone | all-reduce | flops 256 | bytes 2048
  173.9 16.8 %reduce-scatter.9.cloned.1.call-done = f32[64,256]{1,0:T(8,128)} async-done(((f32[256,256]{1,0:T(8,128)}), f32[64,256]{1,0:T(8,128)}) %reduce-scatter.9.cloned.1.call-update) | async-done | bytes 65552 | tf_op jit(solution)/shard_map/reduce_scatter | solution.py:79
  191.7 1.0 fusion
  192.8 1.0 fusion.1
  193.8 0.9 fusion.31
  194.8 0.9 convolution_subtract_fusion
  196.7 5.5 %all_gather.15 = bf16[256,256]{1,0:T(8,128)(2,1)S(1)} all-gather(bf16[64,256]{1,0:T(8,128)(2,1)S(1)} %fusion.71), channel_id=1, replica_groups=mesh['tp'=8,'dp'=4] {'dp'}, dimensions={0}, use_global_device_ids=true | all-gather | bytes 163840 | tf_op jit(solution)/shard_map/all_gather | solution.py:96
  202.7 1.1 pad_maximum_fusion.1
  204.3 1.6 copy.38
  205.9 63.0 %reduce-scatter.11.cloned.1.call-done = f32[32,1024]{1,0:T(8,128)} async-done(((f32[256,1024]{1,0:T(8,128)}), f32[32,1024]{1,0:T(8,128)}) %reduce-scatter.11.cloned.1.call-update) | async-done | bytes 131088 | tf_op jit(solution)/shard_map/reduce_scatter | solution.py:98
  268.9 1.5 fusion.91
  (76 shorter events, 10.9 us)
Async XLA Ops:
  7.2 40.9 %copy-start.2 = (f32[2,64,16,128]{3,2,1,0:T(8,128)S(1)}, f32[2,64,16,128]{3,2,1,0:T(8,128)}, u32[]{:S(2)}) copy-start(f32[2,64,16,128]{3,2,1,0:T(8,128)} %param.27) | copy-start | bytes 3145732
  7.2 54.1 %reduce-scatter.5.cloned.1.call-start = ((), (), s32[]{:S(2)}) async-start(), calls=%async_computation.4 | async-start | bytes 327680 | tf_op jit(solution)/shard_map/reduce_scatter | solution.py:79
  38.5 0.8 copy-start.15
  38.5 0.8 copy-start.16
  38.5 101.0 %reduce-scatter.7.cloned.1.call-start = ((), (), s32[]{:S(2)}) async-start(), calls=%async_computation.5 | async-start | bytes 1179648 | tf_op jit(solution)/shard_map/reduce_scatter | solution.py:98
  38.5 0.7 copy-start.18
  39.5 0.7 copy-start.17
  46.1 0.7 copy-start.19
  48.2 14.2 %copy-start.1 = (f32[2,16,64,16]{2,3,1,0:T(8,128)S(1)}, f32[2,16,64,16]{2,3,1,0:T(8,128)}, u32[]{:S(2)}) copy-start(f32[2,16,64,16]{2,3,1,0:T(8,128)} %param.20) | copy-start | bytes 393220
  48.5 13.8 %copy-start = (f32[2,16,64,16]{2,3,1,0:T(8,128)S(1)}, f32[2,16,64,16]{2,3,1,0:T(8,128)}, u32[]{:S(2)}) copy-start(f32[2,16,64,16]{2,3,1,0:T(8,128)} %param.21) | copy-start | bytes 393220
  63.4 1.1 copy-start.12
  64.5 1.0 copy-start.8
  65.4 7.5 %copy-start.4 = (bf16[2,256,512]{2,1,0:T(8,128)(2,1)S(1)}, bf16[2,256,512]{2,1,0:T(8,128)(2,1)}, u32[]{:S(2)}) copy-start(bf16[2,256,512]{2,1,0:T(8,128)(2,1)} %param.26) | copy-start | bytes 1572868
  66.3 0.9 copy-start.10
  67.3 5.8 %copy-start.6 = (bf16[2,256,512]{2,1,0:T(8,128)(2,1)S(1)}, bf16[2,256,512]{2,1,0:T(8,128)(2,1)}, u32[]{:S(2)}) copy-start(bf16[2,256,512]{2,1,0:T(8,128)(2,1)} %param.25) | copy-start | bytes 1572868
  74.4 65.1 %copy-start.14 = (bf16[32,512]{1,0:T(8,128)(2,1)S(1)}, bf16[32,512]{1,0:T(8,128)(2,1)}, u32[]{:S(2)}) copy-start(bf16[32,512]{1,0:T(8,128)(2,1)} %param.14) | copy-start | bytes 98308
  74.4 92.5 %copy-start.3 = (bf16[2,512,256]{2,1,0:T(8,128)(2,1)S(1)}, bf16[2,512,256]{2,1,0:T(8,128)(2,1)}, u32[]{:S(2)}) copy-start(bf16[2,512,256]{2,1,0:T(8,128)(2,1)} %param.16) | copy-start | bytes 1572868
  74.4 116.3 %reduce-scatter.9.cloned.1.call-start = ((), (), s32[]{:S(2)}) async-start(), calls=%async_computation.6 | async-start | bytes 327680 | tf_op jit(solution)/shard_map/reduce_scatter | solution.py:79
  167.8 101.1 %reduce-scatter.11.cloned.1.call-start = ((), (), s32[]{:S(2)}) async-start(), calls=%async_computation.7 | async-start | bytes 1179648 | tf_op jit(solution)/shard_map/reduce_scatter | solution.py:98
  192.7 1.1 copy-start.13
  193.8 1.0 copy-start.9
  194.8 7.4 %copy-start.5 = (bf16[2,256,512]{2,1,0:T(8,128)(2,1)S(1)}, bf16[2,256,512]{2,1,0:T(8,128)(2,1)}, u32[]{:S(2)}) copy-start(bf16[2,256,512]{2,1,0:T(8,128)(2,1)} %param.26) | copy-start | bytes 1572868
  195.7 0.9 copy-start.11
  196.7 5.8 %copy-start.7 = (bf16[2,256,512]{2,1,0:T(8,128)(2,1)S(1)}, bf16[2,256,512]{2,1,0:T(8,128)(2,1)}, u32[]{:S(2)}) copy-start(bf16[2,256,512]{2,1,0:T(8,128)(2,1)} %param.25) | copy-start | bytes 1572868
Sparse Core Ops, SparseCore 0:
  38.6 22.6 reduce-scatter.4
  74.5 64.8 reduce-scatter.6
  168.0 22.6 reduce-scatter.8
  203.9 64.9 reduce-scatter.10
where the time goes:
time: 279 us; the launch traced here: 277 us
  waiting for transfers between devices  158 us (57%)
  blocking collectives  77.8 us (28%)
  between operations  14.7 us (5%)
  matrix products  11.6 us (4%)
  other arithmetic  7.82 us (3%)
  local copies, waits for them, and re-layouts  7.2 us (3%)
    reduce_scatter x2, waiting for transfers between devices, per_device(): lax.psum_scatter(half_output(mixed_all, w_val[layer_no], w_gate[layer_no]...  128 us
    all_gather x2, blocking collectives, per_device(): gathered = lax.all_gather(stream, 'tp', axis=0, tiled=True)  55.1 us
    reduce_scatter x2, waiting for transfers between devices, per_device(): lax.psum_scatter(partial_value, 'dp', scatter_dimension=0, tiled=True)  29.6 us
    unnamed x2, blocking collectives  11.6 us
    all_gather x2, blocking collectives, per_device(): mixed_all = lax.all_gather(mixed, 'dp', axis=0, tiled=True)  11.1 us
    unnamed x42, local copies, waits for them, and re-layouts  5.66 us
  transfers between devices with their start and end apart: 4, of which 4 were waited for; matrix products, arithmetic and copies ran while one was open for 1% of the time, Pallas kernels for 0%

commit v1 on v0

v1 whole, which is shorter than its diff:
```python
import functools

import jax
import jax.numpy as jnp
from jax import lax
from jax.experimental import pallas as pl
from jax.experimental.pallas import tpu as pltpu
from jax.sharding import PartitionSpec as P

EPS = 1e-06
F32 = jnp.float32
BF16 = jnp.bfloat16
HIGHEST = lax.Precision.HIGHEST
NT = (((1,), (1,)), ((), ()))


def partner(me, k, n, back=False):
    if n & (n - 1):
        return (me + (n - k if back else k)) % n
    found, bit = 0, 1
    while bit < n:
        mine = (me // bit) % 2
        found = found + (bit * (1 - mine) if k & bit else bit * mine)
        bit *= 2
    return found


def kernel(
    tp, dp, chans,
    stream_ref, gain_ref, w_in_hbm, keep_ref, drive_hbm, read_hbm, skip_ref, w_val_hbm, w_gate_hbm, state_hbm,
    out_ref, states_hbm,
    w_in, w_val, w_gate, drive, read, state,
    kept, proj, u_keep, masked, from_old, mix_w,
    x_all, part_send, part_recv, sq_send, sq_recv, mix_all, comb_send, comb_own, comb_recv,
    load_sem, store_sem, x_ss, x_rs, part_ss, part_rs, sq_ss, sq_rs, mix_ss, mix_rs, comb_ss, comb_rs,
):
    layers = w_in.shape[0]
    me_t, me_d = lax.axis_index("tp"), lax.axis_index("dp")
    rows_t, feats = stream_ref.shape
    rows_d, width = u_keep.shape[1:]
    per = rows_d // rows_t
    groups = keep_ref.shape[2]
    lanes = state.shape[2]
    sq_width = sq_send.shape[3]

    loads = {}
    for l in range(layers):
        for i, (src, dst) in enumerate(
            ((state_hbm, state), (drive_hbm, drive), (read_hbm, read), (w_in_hbm, w_in), (w_val_hbm, w_val), (w_gate_hbm, w_gate))
        ):
            loads[l, i] = pltpu.make_async_copy(src.at[l], dst.at[l], load_sem.at[l, i])
            loads[l, i].start()

    barrier = pltpu.get_barrier_semaphore()
    for k in range(1, dp):
        pl.semaphore_signal(barrier, inc=1, device_id={"dp": partner(me_d, k, dp)}, device_id_type=pl.DeviceIdType.MESH)
    for k in range(1, tp):
        pl.semaphore_signal(barrier, inc=1, device_id={"tp": partner(me_t, k, tp)}, device_id_type=pl.DeviceIdType.MESH)

    def send(src, dst, ss, rs, axis, to):
        return pltpu.make_async_remote_copy(
            src_ref=src, dst_ref=dst, send_sem=ss, recv_sem=rs, device_id={axis: to}, device_id_type=pl.DeviceIdType.MESH
        )

    def x_copy(l, k):
        src = stream_ref if l == 0 else x_all.at[l, me_t]
        to = partner(me_t, k, tp)
        return send(src, x_all.at[l, me_t], x_ss.at[l, to], x_rs.at[l, me_t], "tp", to)

    def part_copy(l, to):
        return send(part_send.at[l, to], part_recv.at[l, me_d], part_ss.at[l, to], part_rs.at[l, me_d], "dp", to)

    def sq_copy(l, to):
        return send(sq_send.at[l, to], sq_recv.at[l, me_d], sq_ss.at[l, to], sq_rs.at[l, me_d], "dp", to)

    def mix_copy(l, to):
        return send(mix_all.at[l, me_d], mix_all.at[l, me_d], mix_ss.at[l, to], mix_rs.at[l, me_d], "dp", to)

    def comb_copy(l, to):
        return send(comb_send.at[l, to], comb_recv.at[l, me_t], comb_ss.at[l, to], comb_rs.at[l, me_t], "tp", to)

    def arrival(ref, rs, axis):
        return send(ref, ref, rs, rs, axis, 0)

    lane_group = lax.broadcasted_iota(jnp.int32, (rows_d, width), 1) // chans
    eye = lax.broadcasted_iota(jnp.int32, (rows_d, sq_width), 0) == lax.broadcasted_iota(jnp.int32, (rows_d, sq_width), 1)

    def prepare(l):
        for i in range(3):
            loads[l, i].wait()
        for g in range(groups):
            old = state[l, pl.ds(g, rows_d, stride=groups), :]
            kept[l, pl.ds(g * rows_d, rows_d), :] = (
                keep_ref[l, 0, g : g + 1, :] * old + keep_ref[l, 1, g : g + 1, :] * pltpu.roll(old, lanes // 2, 1)
            )
        proj[...] = lax.dot_general(kept[l], read[l], NT, precision=HIGHEST, preferred_element_type=F32)
        total = jnp.zeros((rows_d, width), F32)
        for g in range(groups):
            total = jnp.where(lane_group == g, proj[pl.ds(g * rows_d, rows_d), :], total)
        from_old[l] = total
        full = lax.dot_general(drive[l], read[l], NT, precision=HIGHEST, preferred_element_type=F32)
        same = (
            lax.broadcasted_iota(jnp.int32, (width, width), 0) // chans
            == lax.broadcasted_iota(jnp.int32, (width, width), 1) // chans
        )
        mix_w[l] = jnp.where(same, full, 0.0)

    def update(l):
        u = u_keep[l]
        for g in range(groups):
            masked[pl.ds(g * rows_d, rows_d), :] = jnp.where(lane_group == g, u, 0.0)
        kept[l] = kept[l] + jnp.dot(masked[...], drive[l], precision=HIGHEST, preferred_element_type=F32)
        for g in range(groups):
            state[l, pl.ds(g, rows_d, stride=groups), :] = kept[l, pl.ds(g * rows_d, rows_d), :]
        pltpu.make_async_copy(state.at[l], states_hbm.at[l], store_sem.at[l]).start()

    pl.semaphore_wait(barrier, tp + dp - 2)
    for k in reversed(range(1, tp)):
        x_copy(0, k).start()
    x_all[0, me_t] = stream_ref[...]
    prepare(0)

    for l in range(layers):
        loads[l, 3].wait()
        gain = gain_ref[l : l + 1, :]
        own_part = own_sq = None
        for k in reversed(range(dp)):
            to = partner(me_d, k, dp)
            for j in range(per):
                t = to * per + j

                @pl.when(t != me_t)
                def _():
                    arrival(x_all.at[l, t], x_rs.at[l, t], "tp").wait_recv()

            x = x_all[l, pl.ds(to * per, per)].astype(F32).reshape(rows_d, feats)
            column = jnp.sum(x * x, axis=1, keepdims=True)
            squares = jnp.sum(jnp.where(eye, column, 0.0), axis=0, keepdims=True)
            product = jnp.dot((x * gain).astype(BF16), w_in[l], preferred_element_type=F32)
            if k:
                sq_send[l, to] = jnp.broadcast_to(squares, (8, sq_width))
                sq_copy(l, to).start()
                part_send[l, to] = product.astype(BF16)
                part_copy(l, to).start()
            else:
                own_part, own_sq = product, squares
        for k in range(1, dp):
            by = partner(me_d, k, dp, True)
            arrival(sq_recv.at[l, by], sq_rs.at[l, by], "dp").wait_recv()
            own_sq = own_sq + sq_recv[l, by][0:1, :]
            arrival(part_recv.at[l, by], part_rs.at[l, by], "dp").wait_recv()
            own_part = own_part + part_recv[l, by].astype(F32)
        square_total = jnp.sum(jnp.where(eye, own_sq, 0.0), axis=1, keepdims=True)
        u = lax.rsqrt(square_total / (feats * dp) + EPS) * own_part
        u_keep[l] = u
        pre = from_old[l] + jnp.dot(u, mix_w[l], precision=HIGHEST, preferred_element_type=F32) + skip_ref[l : l + 1, :] * u
        mix_all[l, me_d] = jax.nn.gelu(pre).astype(BF16)
        for k in reversed(range(1, dp)):
            mix_copy(l, partner(me_d, k, dp)).start()
        loads[l, 4].wait()
        loads[l, 5].wait()
        for k in range(dp):
            by = partner(me_d, k, dp, True)
            if k:
                arrival(mix_all.at[l, by], mix_rs.at[l, by], "dp").wait_recv()
            mixed = mix_all[l, by]
            value = jnp.dot(mixed, w_val[l], preferred_element_type=F32)
            gate = jnp.dot(mixed, w_gate[l], preferred_element_type=F32)
            for j in range(per):
                t = by * per + j
                rows = slice(j * rows_t, (j + 1) * rows_t)

                @pl.when(t != me_t)
                def _():
                    comb_send[l, t, :, :feats] = value[rows].astype(BF16)
                    comb_send[l, t, :, feats:] = gate[rows].astype(BF16)
                    comb_copy(l, t).start()

                @pl.when(t == me_t)
                def _():
                    comb_own[:, :feats] = value[rows]
                    comb_own[:, feats:] = gate[rows]

        update(l)
        if l + 1 < layers:
            prepare(l + 1)
        combined = comb_own[...]
        for k in range(1, tp):
            by = partner(me_t, k, tp, True)
            arrival(comb_recv.at[l, by], comb_rs.at[l, by], "tp").wait_recv()
            combined = combined + comb_recv[l, by].astype(F32)
        fresh = (
            x_all[l, me_t].astype(F32) + combined[:, :feats] * jax.nn.sigmoid(combined[:, feats:])
        ).astype(BF16)
        if l + 1 < layers:
            x_all[l + 1, me_t] = fresh
            for k in reversed(range(1, tp)):
                x_copy(l + 1, k).start()
        else:
            out_ref[...] = fresh

    for l in range(layers):
        for k in range(1, tp):
            x_copy(l, k).wait_send()
            comb_copy(l, partner(me_t, k, tp)).wait_send()
        for k in range(1, dp):
            to = partner(me_d, k, dp)
            part_copy(l, to).wait_send()
            sq_copy(l, to).wait_send()
            mix_copy(l, to).wait_send()
        pltpu.make_async_copy(state.at[l], states_hbm.at[l], store_sem.at[l]).wait()


def per_device(
    tp, dp,
    stream, norm_gain, w_input, lam_re, lam_im, log_dt, b_re, b_im, readout_real, readout_imaginary, d_skip,
    w_val, w_gate, state,
):
    layers, feats, width = w_input.shape
    rows_t = stream.shape[0]
    rows_d, groups, lanes = state.shape[1:]
    chans = b_re.shape[-1]

    step_size = jnp.exp(log_dt)[..., None]
    decay = jnp.exp(lam_re * step_size)
    angle = lam_im * step_size
    keep_re = decay * jnp.cos(angle)
    keep_im = decay * jnp.sin(angle)
    denom = lam_re * lam_re + lam_im * lam_im
    ratio_re = (((keep_re - 1.0) * lam_re + keep_im * lam_im) / denom)[:, :, None, :]
    ratio_im = ((keep_im * lam_re - (keep_re - 1.0) * lam_im) / denom)[:, :, None, :]
    keep = jnp.stack(
        [jnp.concatenate([keep_re, keep_re], -1), jnp.concatenate([-keep_im, keep_im], -1)], axis=1
    )
    turned_re, turned_im = b_re.swapaxes(2, 3), b_im.swapaxes(2, 3)
    drive = jnp.concatenate(
        [ratio_re * turned_re - ratio_im * turned_im, ratio_re * turned_im + ratio_im * turned_re], -1
    ).reshape(layers, width, lanes)
    read = jnp.concatenate([readout_real, -readout_imaginary], -1).reshape(layers, width, lanes)

    vmem = pl.BlockSpec(memory_space=pltpu.VMEM)
    hbm = pl.BlockSpec(memory_space=pl.ANY)
    sq_width = max(rows_d, 128)
    dma = lambda *shape: pltpu.SemaphoreType.DMA(shape)
    out, states = pl.pallas_call(
        functools.partial(kernel, tp, dp, chans),
        out_shape=(
            jax.ShapeDtypeStruct(stream.shape, BF16),
            jax.ShapeDtypeStruct((layers, rows_d * groups, lanes), F32),
        ),
        in_specs=[vmem, vmem, hbm, vmem, hbm, hbm, vmem, hbm, hbm, hbm],
        out_specs=(vmem, hbm),
        scratch_shapes=[
            pltpu.VMEM(w_input.shape, BF16),
            pltpu.VMEM(w_val.shape, BF16),
            pltpu.VMEM(w_gate.shape, BF16),
            pltpu.VMEM(drive.shape, F32),
            pltpu.VMEM(read.shape, F32),
            pltpu.VMEM((layers, rows_d * groups, lanes), F32),
            pltpu.VMEM((layers, rows_d * groups, lanes), F32),
            pltpu.VMEM((rows_d * groups, width), F32),
            pltpu.VMEM((layers, rows_d, width), F32),
            pltpu.VMEM((rows_d * groups, width), F32),
            pltpu.VMEM((layers, rows_d, width), F32),
            pltpu.VMEM((layers, width, width), F32),
            pltpu.VMEM((layers, tp, rows_t, feats), BF16),
            pltpu.VMEM((layers, dp, rows_d, width), BF16),
            pltpu.VMEM((layers, dp, rows_d, width), BF16),
            pltpu.VMEM((layers, dp, 8, sq_width), F32),
            pltpu.VMEM((layers, dp, 8, sq_width), F32),
            pltpu.VMEM((layers, dp, rows_d, width), BF16),
            pltpu.VMEM((layers, tp, rows_t, 2 * feats), BF16),
            pltpu.VMEM((rows_t, 2 * feats), F32),
            pltpu.VMEM((layers, tp, rows_t, 2 * feats), BF16),
            dma(layers, 6), dma(layers),
            dma(layers, tp), dma(layers, tp),
            dma(layers, dp), dma(layers, dp),
            dma(layers, dp), dma(layers, dp),
            dma(layers, dp), dma(layers, dp),
            dma(layers, tp), dma(layers, tp),
        ],
        compiler_params=pltpu.CompilerParams(collective_id=0, has_side_effects=True, vmem_limit_bytes=56 * 1024 * 1024),
    )(
        stream, norm_gain, w_input, keep, drive, read, d_skip, w_val, w_gate,
        state.reshape(layers, rows_d * groups, lanes),
    )
    return out, states.reshape(state.shape)


def solution(mesh):
    return jax.shard_map(
        functools.partial(per_device, mesh.shape["tp"], mesh.shape["dp"]),
        mesh=mesh,
        in_specs=(
            P("tp", "dp"),
            P(None, "dp"),
            P(None, "dp", "tp"),
            P(None, "tp", None),
            P(None, "tp", None),
            P(None, "tp"),
            P(None, "tp", None, None),
            P(None, "tp", None, None),
            P(None, "tp", None, None),
            P(None, "tp", None, None),
            P(None, "tp"),
            P(None, "tp", "dp"),
            P(None, "tp", "dp"),
            P(None, "dp", "tp", None),
        ),
        out_specs=(P("tp", "dp"), P(None, "dp", "tp", None)),
        check_vma=False,
    )
```

time: 279 us -> 69.6 us (0.25)
  waiting for transfers between devices: 158 us -> 0 us
  blocking collectives: 77.8 us -> 0 us
  Pallas kernels: 0 us -> 59.7 us
  between operations: 14.7 us -> 0.66 us
  matrix products: 11.6 us -> 0 us
  other arithmetic: 7.82 us -> 3.36 us
    reduce_scatter x4 -> x0, waiting for transfers between devices: 158 us -> none  [the longest x2 128 us: per_device(): lax.psum_scatter(half_output(mixed_all, w_val[layer_no], w_gate[layer_no]...]
    all_gather x4 -> x0, blocking collectives: 66.2 us -> none  [the longest x2 55.1 us: per_device(): gathered = lax.all_gather(stream, 'tp', axis=0, tiled=True)]
    pallas_call x0 -> x1, Pallas kernels: none -> 59.7 us  [per_device(): pl.pallas_call(functools.partial(kernel, tp, dp, chans), out_shape=(jax.S...]
    unnamed x2 -> x0, blocking collectives: 11.6 us -> none
    dot_general x14 -> x0, matrix products: 11.6 us -> none  [the longest x2 2.83 us: per_device(): jnp.dot(normed, weight_in, preferred_element_type=jnp.float32)]
    unnamed x42 -> x10, local copies, waits for them, and re-layouts: 5.66 us -> 4.76 us
  transfers between devices with their start and end apart: 4 -> 0, of which waited for: 4 -> 0; matrix products, arithmetic and copies ran while one was open for 1% -> 0% of each run, Pallas kernels for 0% -> 0%
where the time goes in v1:
time: 69.6 us; the launch traced here: 69.2 us
  Pallas kernels  59.7 us (86%)
  local copies, waits for them, and re-layouts  5.48 us (8%)
  other arithmetic  3.36 us (5%)
    pallas_call x1, Pallas kernels, per_device(): pl.pallas_call(functools.partial(kernel, tp, dp, chans), out_shape=(jax.S...  59.7 us
    unnamed x10, local copies, waits for them, and re-layouts  4.76 us

profile of v1, /device:TPU:14, one launch (start us, length us, event | category | flops | bytes accessed | tf_op | source)
XLA Modules:
  0.0 69.2 jit_solution(12335487987037700771)
XLA Ops:
  0.6 0.0 copy-start.1
  0.6 0.7 %exp.6 = f32[2,16]{1,0:T(2,128)S(1)} exponential(f32[2,16]{1,0:T(2,128)} %param.19) | non-fusion elementwise | bytes 256 | tf_op jit(solution)/shard_map/exp | solution.py:224
  1.4 0.9 %fusion = (f32[2,16,64]{2,1,0:T(8,128)S(1)}, f32[2,16,64]{2,1,0:T(8,128)S(1)}, f32[2,16,64]{2,1,0:T(8,128)S(1)}, f32[2,16,64]{2,1,0:T(8,128)S(1)}, f32[2,16,64]{2,1,0:T(8,128)S(1)}) fusion(f32[2,16,64]{2,1,0:T(8,128)} %param.18, f32[2,16,64]{2,1,0:T(8,128)} %param.17, f32[2,16]{1,0:T(2,128)S(1)} %exp.6), kind=kLoop, calls=%fused_computation.9 | loop fusion | flops 34816 | bytes 57472 | tf_op jit(solution)/shard_map/div | solution.py:230
  2.3 0.1 maximum_bitcast_fusion
  2.3 0.6 pad_maximum_fusion.2.keep_ref
  3.0 0.0 copy-done.1
  3.0 0.0 copy-start
  3.0 0.9 %copy-done = f32[2,16,16,64]{3,2,1,0:T(8,128)S(1)} copy-done((f32[2,16,16,64]{3,2,1,0:T(8,128)S(1)}, f32[2,16,16,64]{3,2,1,0:T(8,128)}, u32[]{:S(2)}) %copy-start) | copy-done | bytes 131096
  3.9 0.0 copy-start.2
  3.9 0.0 copy-start.3
  3.9 0.8 %pad_maximum_fusion.1 = f32[2,16,16,128]{3,2,1,0:T(8,128)} fusion(f32[2,16,16,64]{3,2,1,0:T(8,128)S(1)} %neg.7, f32[2,16,16,64]{3,2,1,0:T(8,128)S(1)} %copy-done), kind=kLoop, calls=%fused_computation.1 | loop fusion | flops 65536 | bytes 524288 | tf_op jit(solution)/shard_map/concatenate | solution.py:239
  4.8 0.1 copy-done.2
  4.9 0.1 copy-done.3
  4.9 0.1 subtract_bitcast_fusion
  5.0 0.8 %pad_maximum_fusion = f32[2,16,16,128]{3,2,1,0:T(8,128)} fusion(f32[2,16,16,64]{3,2,1,0:T(8,128)S(1)} %get-tuple-element.7, f32[2,16,16,64]{3,2,1,0:T(8,128)S(1)} %get-tuple-element.6), kind=kLoop, calls=%fused_computation | loop fusion | flops 65536 | bytes 524288 | tf_op jit(solution)/shard_map/concatenate | solution.py:236
  5.9 59.7 %shard_map.149 = (bf16[32,512]{1,0:T(8,128)(2,1)}, f32[2,1024,128]{2,1,0:T(8,128)}) custom-call(bf16[32,512]{1,0:T(8,128)(2,1)} %stream_ref.1, f32[2,512]{1,0:T(2,128)} %gain_ref.1, bf16[2,512,256]{2,1,0:T(8,128)(2,1)} %w_in_hbm.1, f32[2,2,16,128]{3,2,1,0:T(8,128)} %pad_maximum_fusion.2.keep_ref, f32[2,256,128]{2,1,0:T(8,128)} %bitcast.17, ...), custom_call_target="tpu_custom_call" | custom-call | tf_op jit(solution)/shard_map/pallas_call | solution.py:245
  65.5 1.4 %copy.19 = bf16[32,512]{1,0:T(8,128)(2,1)} copy(bf16[32,512]{1,0:T(8,128)(2,1)} %get-tuple-element.17) | data formatting | bytes 65536
  66.9 2.3 %copy.20 = f32[2,64,16,128]{3,2,1,0:T(8,128)} copy(f32[2,64,16,128]{3,2,1,0:T(8,128)} %bitcast.15) | data formatting | bytes 2097152
  (1 shorter events, 0.0 us)
Async XLA Ops:
  0.6 2.3 %copy-start.1 = (f32[2,16,16,64]{3,2,1,0:T(8,128)S(1)}, f32[2,16,16,64]{3,2,1,0:T(8,128)}, u32[]{:S(2)}) copy-start(f32[2,16,16,64]{3,2,1,0:T(8,128)} %param.23) | copy-start | bytes 393220
  3.0 1.0 %copy-start = (f32[2,16,16,64]{3,2,1,0:T(8,128)S(1)}, f32[2,16,16,64]{3,2,1,0:T(8,128)}, u32[]{:S(2)}) copy-start(f32[2,16,16,64]{3,2,1,0:T(8,128)} %param.22) | copy-start | bytes 393220
  3.9 0.9 %copy-start.2 = (f32[2,16,64,16]{2,3,1,0:T(8,128)S(1)}, f32[2,16,64,16]{2,3,1,0:T(8,128)}, u32[]{:S(2)}) copy-start(f32[2,16,64,16]{2,3,1,0:T(8,128)} %param.21) | copy-start | bytes 393220
  3.9 1.0 %copy-start.3 = (f32[2,16,64,16]{2,3,1,0:T(8,128)S(1)}, f32[2,16,64,16]{2,3,1,0:T(8,128)}, u32[]{:S(2)}) copy-start(f32[2,16,64,16]{2,3,1,0:T(8,128)} %param.20) | copy-start | bytes 393220

commit v2 on v1

--- a/solution.py
+++ b/solution.py
@@ -27,26 +27,30 @@
 
 def kernel(
     tp, dp, chans,
-    stream_ref, gain_ref, w_in_hbm, keep_ref, drive_hbm, read_hbm, skip_ref, w_val_hbm, w_gate_hbm, state_hbm,
-    out_ref, states_hbm,
-    w_in, w_val, w_gate, drive, read, state,
+    stream_ref, gain_ref, w_in_hbm, lam_re_ref, lam_im_ref, log_dt_ref, b_re_hbm, b_im_hbm, c_re_hbm, c_im_hbm, skip_ref,
+    w_val_hbm, w_gate_hbm, state_hbm,
+    out_ref, state,
+    w_in, w_val, w_gate, b_re, b_im, c_re, c_im, drive, read,
     kept, proj, u_keep, masked, from_old, mix_w,
     x_all, part_send, part_recv, sq_send, sq_recv, mix_all, comb_send, comb_own, comb_recv,
-    load_sem, store_sem, x_ss, x_rs, part_ss, part_rs, sq_ss, sq_rs, mix_ss, mix_rs, comb_ss, comb_rs,
+    load_sem, x_ss, x_rs, part_ss, part_rs, sq_ss, sq_rs, mix_ss, mix_rs, comb_ss, comb_rs,
 ):
     layers = w_in.shape[0]
     me_t, me_d = lax.axis_index("tp"), lax.axis_index("dp")
     rows_t, feats = stream_ref.shape
     rows_d, width = u_keep.shape[1:]
     per = rows_d // rows_t
-    groups = keep_ref.shape[2]
+    groups, half = lam_re_ref.shape[1:]
     lanes = state.shape[2]
     sq_width = sq_send.shape[3]
 
     loads = {}
     for l in range(layers):
         for i, (src, dst) in enumerate(
-            ((state_hbm, state), (drive_hbm, drive), (read_hbm, read), (w_in_hbm, w_in), (w_val_hbm, w_val), (w_gate_hbm, w_gate))
+            (
+                (b_re_hbm, b_re), (b_im_hbm, b_im), (c_re_hbm, c_re), (c_im_hbm, c_im), (state_hbm, state),
+                (w_in_hbm, w_in), (w_val_hbm, w_val), (w_gate_hbm, w_gate),
+            )
         ):
             loads[l, i] = pltpu.make_async_copy(src.at[l], dst.at[l], load_sem.at[l, i])
             loads[l, i].start()
@@ -85,13 +89,33 @@
     lane_group = lax.broadcasted_iota(jnp.int32, (rows_d, width), 1) // chans
     eye = lax.broadcasted_iota(jnp.int32, (rows_d, sq_width), 0) == lax.broadcasted_iota(jnp.int32, (rows_d, sq_width), 1)
 
+    group_eye = lax.broadcasted_iota(jnp.int32, (groups, groups), 0) == lax.broadcasted_iota(jnp.int32, (groups, groups), 1)
+
     def prepare(l):
-        for i in range(3):
+        step_size = jnp.exp(jnp.sum(jnp.where(group_eye, log_dt_ref[l : l + 1, :], 0.0), axis=1, keepdims=True))
+        lam_re, lam_im = lam_re_ref[l], lam_im_ref[l]
+        decay = jnp.exp(lam_re * step_size)
+        angle = lam_im * step_size
+        keep_re = decay * jnp.cos(angle)
+        keep_im = decay * jnp.sin(angle)
+        denom = lam_re * lam_re + lam_im * lam_im
+        ratio_re = ((keep_re - 1.0) * lam_re + keep_im * lam_im) / denom
+        ratio_im = (keep_im * lam_re - (keep_re - 1.0) * lam_im) / denom
+        keep_a = jnp.concatenate([keep_re, keep_re], axis=1)
+        keep_b = jnp.concatenate([-keep_im, keep_im], axis=1)
+        for i in range(5):
             loads[l, i].wait()
+        for g in range(groups):
+            t_re, t_im = b_re[l, g], b_im[l, g]
+            r_re, r_im = ratio_re[g : g + 1, :], ratio_im[g : g + 1, :]
+            drive[l, pl.ds(g * chans, chans), :] = jnp.concatenate(
+                [r_re * t_re - r_im * t_im, r_re * t_im + r_im * t_re], axis=1
+            )
+        read[l] = jnp.concatenate([c_re[l].reshape(width, half), -c_im[l].reshape(width, half)], axis=1)
         for g in range(groups):
             old = state[l, pl.ds(g, rows_d, stride=groups), :]
             kept[l, pl.ds(g * rows_d, rows_d), :] = (
-                keep_ref[l, 0, g : g + 1, :] * old + keep_ref[l, 1, g : g + 1, :] * pltpu.roll(old, lanes // 2, 1)
+                keep_a[g : g + 1, :] * old + keep_b[g : g + 1, :] * pltpu.roll(old, lanes // 2, 1)
             )
         proj[...] = lax.dot_general(kept[l], read[l], NT, precision=HIGHEST, preferred_element_type=F32)
         total = jnp.zeros((rows_d, width), F32)
@@ -112,7 +136,6 @@
         kept[l] = kept[l] + jnp.dot(masked[...], drive[l], precision=HIGHEST, preferred_element_type=F32)
         for g in range(groups):
             state[l, pl.ds(g, rows_d, stride=groups), :] = kept[l, pl.ds(g * rows_d, rows_d), :]
-        pltpu.make_async_copy(state.at[l], states_hbm.at[l], store_sem.at[l]).start()
 
     pl.semaphore_wait(barrier, tp + dp - 2)
     for k in reversed(range(1, tp)):
@@ -121,7 +144,7 @@
     prepare(0)
 
     for l in range(layers):
-        loads[l, 3].wait()
+        loads[l, 5].wait()
         gain = gain_ref[l : l + 1, :]
         own_part = own_sq = None
         for k in reversed(range(dp)):
@@ -157,8 +180,8 @@
         mix_all[l, me_d] = jax.nn.gelu(pre).astype(BF16)
         for k in reversed(range(1, dp)):
             mix_copy(l, partner(me_d, k, dp)).start()
-        loads[l, 4].wait()
-        loads[l, 5].wait()
+        loads[l, 6].wait()
+        loads[l, 7].wait()
         for k in range(dp):
             by = partner(me_d, k, dp, True)
             if k:
@@ -208,7 +231,6 @@
             part_copy(l, to).wait_send()
             sq_copy(l, to).wait_send()
             mix_copy(l, to).wait_send()
-        pltpu.make_async_copy(state.at[l], states_hbm.at[l], store_sem.at[l]).wait()
 
 
 def per_device(
@@ -221,42 +243,28 @@
     rows_d, groups, lanes = state.shape[1:]
     chans = b_re.shape[-1]
 
-    step_size = jnp.exp(log_dt)[..., None]
-    decay = jnp.exp(lam_re * step_size)
-    angle = lam_im * step_size
-    keep_re = decay * jnp.cos(angle)
-    keep_im = decay * jnp.sin(angle)
-    denom = lam_re * lam_re + lam_im * lam_im
-    ratio_re = (((keep_re - 1.0) * lam_re + keep_im * lam_im) / denom)[:, :, None, :]
-    ratio_im = ((keep_im * lam_re - (keep_re - 1.0) * lam_im) / denom)[:, :, None, :]
-    keep = jnp.stack(
-        [jnp.concatenate([keep_re, keep_re], -1), jnp.concatenate([-keep_im, keep_im], -1)], axis=1
-    )
     turned_re, turned_im = b_re.swapaxes(2, 3), b_im.swapaxes(2, 3)
-    drive = jnp.concatenate(
-        [ratio_re * turned_re - ratio_im * turned_im, ratio_re * turned_im + ratio_im * turned_re], -1
-    ).reshape(layers, width, lanes)
-    read = jnp.concatenate([readout_real, -readout_imaginary], -1).reshape(layers, width, lanes)
-
+
+    limit = 67043328 - 4 * layers * rows_d * groups * lanes - (256 << 10)
     vmem = pl.BlockSpec(memory_space=pltpu.VMEM)
-    hbm = pl.BlockSpec(memory_space=pl.ANY)
+    hbm = pl.BlockSpec(memory_space=pltpu.HBM)
     sq_width = max(rows_d, 128)
     dma = lambda *shape: pltpu.SemaphoreType.DMA(shape)
     out, states = pl.pallas_call(
         functools.partial(kernel, tp, dp, chans),
-        out_shape=(
-            jax.ShapeDtypeStruct(stream.shape, BF16),
-            jax.ShapeDtypeStruct((layers, rows_d * groups, lanes), F32),
-        ),
-        in_specs=[vmem, vmem, hbm, vmem, hbm, hbm, vmem, hbm, hbm, hbm],
-        out_specs=(vmem, hbm),
+        out_shape=(pltpu.VMEM(stream.shape, BF16), pltpu.VMEM((layers, rows_d * groups, lanes), F32)),
+        in_specs=[vmem, vmem, hbm, vmem, vmem, vmem, hbm, hbm, hbm, hbm, vmem, hbm, hbm, hbm],
+        out_specs=(vmem, vmem),
         scratch_shapes=[
             pltpu.VMEM(w_input.shape, BF16),
             pltpu.VMEM(w_val.shape, BF16),
             pltpu.VMEM(w_gate.shape, BF16),
-            pltpu.VMEM(drive.shape, F32),
-            pltpu.VMEM(read.shape, F32),
-            pltpu.VMEM((layers, rows_d * groups, lanes), F32),
+            pltpu.VMEM(turned_re.shape, F32),
+            pltpu.VMEM(turned_im.shape, F32),
+            pltpu.VMEM(readout_real.shape, F32),
+            pltpu.VMEM(readout_imaginary.shape, F32),
+            pltpu.VMEM((layers, width, lanes), F32),
+            pltpu.VMEM((layers, width, lanes), F32),
             pltpu.VMEM((layers, rows_d * groups, lanes), F32),
             pltpu.VMEM((rows_d * groups, width), F32),
             pltpu.VMEM((layers, rows_d, width), F32),
@@ -272,16 +280,17 @@
             pltpu.VMEM((layers, tp, rows_t, 2 * feats), BF16),
             pltpu.VMEM((rows_t, 2 * feats), F32),
             pltpu.VMEM((layers, tp, rows_t, 2 * feats), BF16),
-            dma(layers, 6), dma(layers),
+            dma(layers, 8),
             dma(layers, tp), dma(layers, tp),
             dma(layers, dp), dma(layers, dp),
             dma(layers, dp), dma(layers, dp),
             dma(layers, dp), dma(layers, dp),
             dma(layers, tp), dma(layers, tp),
         ],
-        compiler_params=pltpu.CompilerParams(collective_id=0, has_side_effects=True, vmem_limit_bytes=56 * 1024 * 1024),
+        compiler_params=pltpu.CompilerParams(collective_id=0, has_side_effects=True, vmem_limit_bytes=limit),
     )(
-        stream, norm_gain, w_input, keep, drive, read, d_skip, w_val, w_gate,
+        stream, norm_gain, w_input, lam_re, lam_im, log_dt, turned_re, turned_im, readout_real,
+        readout_imaginary, d_skip, w_val, w_gate,
         state.reshape(layers, rows_d * groups, lanes),
     )
     return out, states.reshape(state.shape)

time: 69.6 us -> 61.6 us (0.89)
  local copies, waits for them, and re-layouts: 5.48 us -> 1.59 us
  other arithmetic: 3.36 us -> 0 us
    unnamed x10 -> x2, local copies, waits for them, and re-layouts: 4.76 us -> 1.59 us
    concatenate x2 -> x0, other arithmetic: 1.68 us -> none  [the longest x1 0.84 us: per_device(): jnp.concatenate([ratio_re * turned_re - ratio_im * turned_im, ratio_re *...]
    div x1 -> x0, other arithmetic: 0.89 us -> none  [per_device(): ((keep_re - 1.0) * lam_re + keep_im * lam_im) / denom]
    exp x1 -> x0, local copies, waits for them, and re-layouts: 0.72 us -> none  [per_device(): step_size = jnp.exp(log_dt)[..., None]]
    another operation x2 -> x0, other arithmetic: 0.7 us -> none  [per_device(): jnp.stack([jnp.concatenate([keep_re, keep_re], -1), jnp.concatenate([-kee...]
where the time goes in v2:
time: 61.6 us; the launch traced here: 61.4 us
  Pallas kernels  59.1 us (96%)
  local copies, waits for them, and re-layouts  1.59 us (3%)
  between operations  0.64 us (1%)
    pallas_call x1, Pallas kernels, per_device(): pl.pallas_call(functools.partial(kernel, tp, dp, chans), out_shape=(pltpu...  59.1 us
    unnamed x2, local copies, waits for them, and re-layouts  1.59 us

profile of v2, /device:TPU:14, one launch (start us, length us, event | category | flops | bytes accessed | tf_op | source)
XLA Modules:
  0.0 61.4 jit_solution(4043450925728364772)
XLA Ops:
  0.6 59.1 %shard_map.149 = (bf16[32,512]{1,0:T(8,128)(2,1)S(1)}, f32[2,1024,128]{2,1,0:T(8,128)S(1)}) custom-call(bf16[32,512]{1,0:T(8,128)(2,1)} %stream_ref.1, f32[2,512]{1,0:T(2,128)} %gain_ref.1, bf16[2,512,256]{2,1,0:T(8,128)(2,1)} %w_in_hbm.1, f32[2,16,64]{2,1,0:T(8,128)} %lam_re_ref.1, f32[2,16,64]{2,1,0:T(8,128)} %lam_im_ref.1, f32[2,16]{1,0:T(2,128)} %log_dt_ref.1, ...), custom_call_target="tpu_custom_call" | custom-call | tf_op jit(solution)/shard_map/pallas_call | solution.py:253
  59.8 0.6 %copy.18 = bf16[32,512]{1,0:T(8,128)(2,1)} copy(bf16[32,512]{1,0:T(8,128)(2,1)S(1)} %get-tuple-element.6) | data formatting | bytes 65536
  60.4 1.0 %copy.19 = f32[2,64,16,128]{3,2,1,0:T(8,128)} copy(f32[2,64,16,128]{3,2,1,0:T(8,128)S(1)} %bitcast.4) | data formatting | bytes 2097152

commit v3 on v2

--- a/solution.py
+++ b/solution.py
@@ -32,14 +32,15 @@
     out_ref, state,
     w_in, w_val, w_gate, b_re, b_im, c_re, c_im, drive, read,
     kept, proj, u_keep, masked, from_old, mix_w,
-    x_all, part_send, part_recv, sq_send, sq_recv, mix_all, comb_send, comb_own, comb_recv,
-    load_sem, x_ss, x_rs, part_ss, part_rs, sq_ss, sq_rs, mix_ss, mix_rs, comb_ss, comb_rs,
+    x_all, part_send, part_recv, sq_send, sq_recv, mix_all, block, comb_send, comb_own, pair_recv, comb_recv,
+    load_sem, x_ss, x_rs, part_ss, part_rs, sq_ss, sq_rs, mix_ss, mix_rs, pair_ss, pair_rs, comb_ss, comb_rs,
 ):
     layers = w_in.shape[0]
     me_t, me_d = lax.axis_index("tp"), lax.axis_index("dp")
     rows_t, feats = stream_ref.shape
     rows_d, width = u_keep.shape[1:]
     per = rows_d // rows_t
+    me_p, side = me_t // 2, me_t % 2
     groups, half = lam_re_ref.shape[1:]
     lanes = state.shape[2]
     sq_width = sq_send.shape[3]
@@ -81,7 +82,14 @@
         return send(mix_all.at[l, me_d], mix_all.at[l, me_d], mix_ss.at[l, to], mix_rs.at[l, me_d], "dp", to)
 
     def comb_copy(l, to):
-        return send(comb_send.at[l, to], comb_recv.at[l, me_t], comb_ss.at[l, to], comb_rs.at[l, me_t], "tp", to)
+        return send(
+            comb_send.at[l, 2 * to + side], comb_recv.at[l, me_p], comb_ss.at[l, to], comb_rs.at[l, me_p], "tp", 2 * to + side
+        )
+
+    def pair_copy(l, q):
+        return send(
+            comb_send.at[l, 2 * q + 1 - side], pair_recv.at[l, q], pair_ss.at[l, q], pair_rs.at[l, q], "tp", 2 * me_p + 1 - side
+        )
 
     def arrival(ref, rs, axis):
         return send(ref, ref, rs, rs, axis, 0)
@@ -182,6 +190,22 @@
             mix_copy(l, partner(me_d, k, dp)).start()
         loads[l, 6].wait()
         loads[l, 7].wait()
+
+        def pass_on(by):
+            for m in range(per // 2):
+                q = by * (per // 2) + m
+                arrival(pair_recv.at[l, q], pair_rs.at[l, q], "tp").wait_recv()
+                total = block[2 * q + side] + pair_recv[l, q].astype(F32)
+
+                @pl.when(q != me_p)
+                def _():
+                    comb_send[l, 2 * q + side] = total.astype(BF16)
+                    comb_copy(l, q).start()
+
+                @pl.when(q == me_p)
+                def _():
+                    comb_own[...] = total
+
         for k in range(dp):
             by = partner(me_d, k, dp, True)
             if k:
@@ -190,26 +214,23 @@
             value = jnp.dot(mixed, w_val[l], preferred_element_type=F32)
             gate = jnp.dot(mixed, w_gate[l], preferred_element_type=F32)
             for j in range(per):
-                t = by * per + j
                 rows = slice(j * rows_t, (j + 1) * rows_t)
-
-                @pl.when(t != me_t)
-                def _():
-                    comb_send[l, t, :, :feats] = value[rows].astype(BF16)
-                    comb_send[l, t, :, feats:] = gate[rows].astype(BF16)
-                    comb_copy(l, t).start()
-
-                @pl.when(t == me_t)
-                def _():
-                    comb_own[:, :feats] = value[rows]
-                    comb_own[:, feats:] = gate[rows]
+                block[by * per + j, :, :feats] = value[rows]
+                block[by * per + j, :, feats:] = gate[rows]
+            for m in range(per // 2):
+                q = by * (per // 2) + m
+                comb_send[l, 2 * q + 1 - side] = block[2 * q + 1 - side].astype(BF16)
+                pair_copy(l, q).start()
+            if k:
+                pass_on(partner(me_d, k - 1, dp, True))
+        pass_on(partner(me_d, dp - 1, dp, True))
 
         update(l)
         if l + 1 < layers:
             prepare(l + 1)
         combined = comb_own[...]
-        for k in range(1, tp):
-            by = partner(me_t, k, tp, True)
+        for k in range(1, tp // 2):
+            by = partner(me_p, k, tp // 2, True)
             arrival(comb_recv.at[l, by], comb_rs.at[l, by], "tp").wait_recv()
             combined = combined + comb_recv[l, by].astype(F32)
         fresh = (
@@ -225,7 +246,10 @@
     for l in range(layers):
         for k in range(1, tp):
             x_copy(l, k).wait_send()
-            comb_copy(l, partner(me_t, k, tp)).wait_send()
+        for k in range(1, tp // 2):
+            comb_copy(l, partner(me_p, k, tp // 2)).wait_send()
+        for q in range(tp // 2):
+            pair_copy(l, q).wait_send()
         for k in range(1, dp):
             to = partner(me_d, k, dp)
             part_copy(l, to).wait_send()
@@ -277,15 +301,18 @@
             pltpu.VMEM((layers, dp, 8, sq_width), F32),
             pltpu.VMEM((layers, dp, 8, sq_width), F32),
             pltpu.VMEM((layers, dp, rows_d, width), BF16),
+            pltpu.VMEM((tp, rows_t, 2 * feats), F32),
             pltpu.VMEM((layers, tp, rows_t, 2 * feats), BF16),
             pltpu.VMEM((rows_t, 2 * feats), F32),
-            pltpu.VMEM((layers, tp, rows_t, 2 * feats), BF16),
+            pltpu.VMEM((layers, tp // 2, rows_t, 2 * feats), BF16),
+            pltpu.VMEM((layers, tp // 2, rows_t, 2 * feats), BF16),
             dma(layers, 8),
             dma(layers, tp), dma(layers, tp),
             dma(layers, dp), dma(layers, dp),
             dma(layers, dp), dma(layers, dp),
             dma(layers, dp), dma(layers, dp),
-            dma(layers, tp), dma(layers, tp),
+            dma(layers, tp // 2), dma(layers, tp // 2),
+            dma(layers, tp // 2), dma(layers, tp // 2),
         ],
         compiler_params=pltpu.CompilerParams(collective_id=0, has_side_effects=True, vmem_limit_bytes=limit),
     )(

time: 61.6 us -> 58.6 us (0.951)
  the two profiles are of different devices: /device:TPU:14 before, /device:TPU:3 now
where the time goes in v3:
time: 58.6 us; the launch traced here: 58.4 us
  Pallas kernels  56.2 us (96%)
  local copies, waits for them, and re-layouts  1.59 us (3%)
  between operations  0.64 us (1%)
    pallas_call x1, Pallas kernels, per_device(): pl.pallas_call(functools.partial(kernel, tp, dp, chans), out_shape=(pltpu...  56.2 us
    unnamed x2, local copies, waits for them, and re-layouts  1.59 us

profile of v3, /device:TPU:3, one launch (start us, length us, event | category | flops | bytes accessed | tf_op | source)
XLA Modules:
  0.0 58.4 jit_solution(3300157701294084868)
XLA Ops:
  0.6 56.2 %shard_map.149 = (bf16[32,512]{1,0:T(8,128)(2,1)S(1)}, f32[2,1024,128]{2,1,0:T(8,128)S(1)}) custom-call(bf16[32,512]{1,0:T(8,128)(2,1)} %stream_ref.1, f32[2,512]{1,0:T(2,128)} %gain_ref.1, bf16[2,512,256]{2,1,0:T(8,128)(2,1)} %w_in_hbm.1, f32[2,16,64]{2,1,0:T(8,128)} %lam_re_ref.1, f32[2,16,64]{2,1,0:T(8,128)} %lam_im_ref.1, f32[2,16]{1,0:T(2,128)} %log_dt_ref.1, ...), custom_call_target="tpu_custom_call" | custom-call | tf_op jit(solution)/shard_map/pallas_call | solution.py:277
  56.8 0.6 %copy.18 = bf16[32,512]{1,0:T(8,128)(2,1)} copy(bf16[32,512]{1,0:T(8,128)(2,1)S(1)} %get-tuple-element.6) | data formatting | bytes 65536
  57.4 1.0 %copy.19 = f32[2,64,16,128]{3,2,1,0:T(8,128)} copy(f32[2,64,16,128]{3,2,1,0:T(8,128)S(1)} %bitcast.4) | data formatting | bytes 2097152

commit v4 on v3

--- a/solution.py
+++ b/solution.py
@@ -221,9 +221,10 @@
                 q = by * (per // 2) + m
                 comb_send[l, 2 * q + 1 - side] = block[2 * q + 1 - side].astype(BF16)
                 pair_copy(l, q).start()
-            if k:
-                pass_on(partner(me_d, k - 1, dp, True))
-        pass_on(partner(me_d, dp - 1, dp, True))
+            if k > 1:
+                pass_on(partner(me_d, k - 2, dp, True))
+        for k in range(max(dp - 2, 0), dp):
+            pass_on(partner(me_d, k, dp, True))
 
         update(l)
         if l + 1 < layers:

time: 58.6 us -> 56.3 us (0.961)
  Pallas kernels: 56.2 us -> 53.9 us
    pallas_call x1, Pallas kernels: 56.2 us -> 53.9 us  [per_device(): pl.pallas_call(functools.partial(kernel, tp, dp, chans), out_shape=(pltpu...]
where the time goes in v4:
time: 56.3 us; the launch traced here: 56.1 us
  Pallas kernels  53.9 us (96%)
  local copies, waits for them, and re-layouts  1.59 us (3%)
  between operations  0.64 us (1%)
    pallas_call x1, Pallas kernels, per_device(): pl.pallas_call(functools.partial(kernel, tp, dp, chans), out_shape=(pltpu...  53.9 us
    unnamed x2, local copies, waits for them, and re-layouts  1.59 us

profile of v4, /device:TPU:3, one launch (start us, length us, event | category | flops | bytes accessed | tf_op | source)
XLA Modules:
  0.0 56.1 jit_solution(12178747258190127167)
XLA Ops:
  0.6 53.9 %shard_map.149 = (bf16[32,512]{1,0:T(8,128)(2,1)S(1)}, f32[2,1024,128]{2,1,0:T(8,128)S(1)}) custom-call(bf16[32,512]{1,0:T(8,128)(2,1)} %stream_ref.1, f32[2,512]{1,0:T(2,128)} %gain_ref.1, bf16[2,512,256]{2,1,0:T(8,128)(2,1)} %w_in_hbm.1, f32[2,16,64]{2,1,0:T(8,128)} %lam_re_ref.1, f32[2,16,64]{2,1,0:T(8,128)} %lam_im_ref.1, f32[2,16]{1,0:T(2,128)} %log_dt_ref.1, ...), custom_call_target="tpu_custom_call" | custom-call | tf_op jit(solution)/shard_map/pallas_call | solution.py:278
  54.5 0.6 %copy.18 = bf16[32,512]{1,0:T(8,128)(2,1)} copy(bf16[32,512]{1,0:T(8,128)(2,1)S(1)} %get-tuple-element.6) | data formatting | bytes 65536
  55.1 1.0 %copy.19 = f32[2,64,16,128]{3,2,1,0:T(8,128)} copy(f32[2,64,16,128]{3,2,1,0:T(8,128)S(1)} %bitcast.4) | data formatting | bytes 2097152
